TPU v7x, 32 devices: a whole 2x2x4 slice. The times are simulated.
32 devices in a mesh: sp: 8 (over z, y), tp: 4 (over x, core).
Axes of the slice: x: 2, y: 2, z: 4, core: 2. Of those that a mesh axis runs over, the one named last changes fastest.
Arguments:
- tokens: bfloat16 [3072, 4096], P(('sp', 'tp')), may hold values from -6 to 6
- norm_gain: float32 [4096], replicated, may hold values from 0.1 to 1.9
- w_query: bfloat16 [4096, 2048], P('sp', 'tp'), may hold values from -0.09375 to 0.09375
- w_key: bfloat16 [4096, 512], P('sp', 'tp'), may hold values from -1.5 to 1.5
- w_value: bfloat16 [4096, 512], P('sp', 'tp'), may hold values from -0.09375 to 0.09375
- w_mem_query: bfloat16 [4096, 1024], P('sp', 'tp'), may hold values from -0.09375 to 0.09375
- w_mem_key: bfloat16 [4096, 1024], P('sp', 'tp'), may hold values from -0.09375 to 0.09375
- w_mem_value: bfloat16 [4096, 1024], P('sp', 'tp'), may hold values from -0.09375 to 0.09375
- w_mem_gate: bfloat16 [4096, 1024], P('sp', 'tp'), may hold values from -0.09375 to 0.09375
- w_gates: bfloat16 [4096, 2, 16], replicated, may hold values from -0.09375 to 0.09375
- sinks: float32 [32], P('tp'), may hold values from 2 to 6
- forget_bias: float32 [16], P('tp'), may hold values from 3 to 13
- forget_shift: float32 [3072, 16], P('sp', 'tp'), may hold values from -1 to 0
- w_out: bfloat16 [3072, 4096], P('sp', 'tp'), may hold values from -0.21650635 to 0.21650635
Outputs:
- mixed: bfloat16 [3072, 4096], P('sp', 'tp')
- log_total: float32 [3072, 32], P('sp', 'tp')
All inputs are finite; a program needn't handle non-finite values.
Results may differ from a plain program's by a relative error of at most 0.018.
Values may be sent and summed in bfloat16 or wider, within the bound.
A program may use at most 128 MiB of HBM per device.

v0:
```python
import math
import jax
import jax.numpy as jnp
from jax import lax
from jax.sharding import PartitionSpec as P

HD = 64
WINDOW = 128
BLK = 128
EPSILON = 1e-06
MASKED = -1e30
exact_precision = lax.Precision.HIGHEST


def passed_along(block, axis, distance):
    devices = range(lax.axis_size(axis))
    route = [(i - distance, i) for i in devices if i - distance in devices]
    return lax.ppermute(block, axis, route)


def entering(x, axis, join, neutral):
    place = lax.axis_index(axis)
    gathered = jax.tree.map(
        lambda a, kind: lax.all_gather(a.astype(kind), axis),
        x,
        (jnp.bfloat16, jnp.bfloat16, jnp.bfloat16, jnp.bfloat16),
    )
    state = jax.tree.map(lambda a, e: jnp.zeros_like(a) + jnp.asarray(e, a.dtype), x, neutral)

    def one(turn, state):
        return join(
            state,
            jax.tree.map(
                lambda a, own: lax.dynamic_index_in_dim(a, turn, 0, False).astype(own.dtype),
                gathered,
                x,
            ),
        )

    return lax.fori_loop(0, place, one, state)


def normalize(tokens, norm_gain):
    values = tokens.astype(jnp.float32)
    rescale = lax.rsqrt(jnp.mean(values * values, axis=-1, keepdims=True) + EPSILON)
    return (values * rescale * norm_gain).astype(jnp.bfloat16)


def advance(carried, key_block, value_block, in_block, cumulative):
    memory_state, normalizer, stabilizer = carried
    block_total = cumulative[:, -1]
    decays = block_total[:, None] - cumulative + in_block
    new_stabilizer = jnp.maximum(block_total + stabilizer, jnp.max(decays, axis=-1))
    weights = jnp.exp(decays - new_stabilizer[:, None])
    rescale = jnp.exp(block_total + stabilizer - new_stabilizer)
    new_state = rescale[:, None, None] * memory_state + jnp.einsum(
        "hsv,hsk->hvk", value_block * weights[:, :, None], key_block, precision=exact_precision
    )
    new_normalizer = rescale[:, None] * normalizer + jnp.einsum(
        "hs,hsk->hk", weights, key_block, precision=exact_precision
    )
    return (new_state, new_normalizer, new_stabilizer)


def block_step(carried, block_data):
    memory_state, normalizer, stabilizer = carried
    query_block, key_block, value_block, in_block, forget_block = block_data
    length = in_block.shape[-1]
    cumulative = jnp.cumsum(forget_block, axis=-1)
    causal = lax.broadcasted_iota(jnp.int32, (length, length), 0) >= lax.broadcasted_iota(
        jnp.int32, (length, length), 1
    )
    log_weight = jnp.where(
        causal[None], cumulative[:, :, None] - cumulative[:, None, :] + in_block[:, None, :], MASKED
    )
    row_level = jnp.maximum(cumulative + stabilizer[:, None], jnp.max(log_weight, axis=-1))
    carried_part = jnp.exp(cumulative + stabilizer[:, None] - row_level)
    affinity = jnp.einsum(
        "htd,hsd->hts", query_block, key_block, precision=exact_precision
    ) * jnp.exp(log_weight - row_level[:, :, None])
    numerator = carried_part[:, :, None] * jnp.einsum(
        "hvk,htk->htv", memory_state, query_block, precision=exact_precision
    ) + jnp.einsum("hts,hsv->htv", affinity, value_block, precision=exact_precision)
    denominator = carried_part * jnp.einsum(
        "hk,htk->ht", normalizer, query_block, precision=exact_precision
    ) + jnp.sum(affinity, axis=-1)
    recall = numerator / jnp.maximum(jnp.abs(denominator), jnp.exp(-row_level))[:, :, None]
    return (advance(carried, key_block, value_block, in_block, cumulative), recall)


def join_states(earlier, later):
    passed_one, state_one, normal_one, level_one = earlier
    passed_two, state_two, normal_two, level_two = later
    new_level = jnp.maximum(passed_two + level_one, level_two)
    weight_one = jnp.exp(passed_two + level_one - new_level)
    weight_two = jnp.exp(level_two - new_level)
    new_state = weight_one[:, None, None] * state_one + weight_two[:, None, None] * state_two
    new_normal = weight_one[:, None] * normal_one + weight_two[:, None] * normal_two
    return (passed_one + passed_two, new_state, new_normal, new_level)


def attend(query, key_rows, value_rows, sinks):
    row_count = query.shape[0]
    kv_local = key_rows.shape[1] // HD
    group_size = query.shape[1] // HD // kv_local
    block_count = row_count // WINDOW
    rim_key, rim_value = passed_along(
        (key_rows[row_count - WINDOW :], value_rows[row_count - WINDOW :]), "sp", 1
    )
    padded_keys = jnp.concatenate([rim_key, key_rows], axis=0).reshape(
        block_count + 1, WINDOW, kv_local, HD
    )
    padded_values = jnp.concatenate([rim_value, value_rows], axis=0).reshape(
        block_count + 1, WINDOW, kv_local, HD
    )
    key_window = jnp.concatenate([padded_keys[:-1], padded_keys[1:]], axis=1)
    value_window = jnp.concatenate([padded_values[:-1], padded_values[1:]], axis=1)
    q_blocks = query.reshape(block_count, WINDOW, kv_local, group_size, HD)
    scores = jnp.einsum(
        "nqhgd,nkhd->nhgqk", q_blocks, key_window, preferred_element_type=jnp.float32
    ) * HD ** (-0.5)
    query_index = lax.broadcasted_iota(jnp.int32, (WINDOW, 2 * WINDOW), 0)
    key_index = lax.broadcasted_iota(jnp.int32, (WINDOW, 2 * WINDOW), 1)
    distance = query_index - key_index + WINDOW
    in_band = (distance >= 0) & (distance < WINDOW)
    block_index = lax.broadcasted_iota(jnp.int32, (block_count, WINDOW, 2 * WINDOW), 0)
    key_position = (
        lax.axis_index("sp") * row_count + block_index * WINDOW - WINDOW + key_index[None]
    )
    allowed = (in_band[None] & (key_position >= 0))[:, None, None]
    scores = jnp.where(allowed, scores, MASKED)
    sink_logit = sinks.reshape(1, kv_local, group_size, 1, 1)
    ceiling = jnp.maximum(jnp.max(scores, axis=-1, keepdims=True), sink_logit)
    weights = jnp.exp(scores - ceiling)
    partition = jnp.exp(sink_logit - ceiling) + jnp.sum(weights, axis=-1, keepdims=True)
    log_total = (
        (ceiling + jnp.log(partition))[..., 0]
        .transpose(0, 3, 1, 2)
        .reshape(row_count, kv_local * group_size)
    )
    probs = (weights / partition).astype(jnp.bfloat16)
    head_out = jnp.einsum(
        "nhgqk,nkhd->nqhgd", probs, value_window, preferred_element_type=jnp.float32
    )
    return (head_out.astype(jnp.bfloat16).reshape(row_count, kv_local * group_size * HD), log_total)


def memory(mem_query, mem_key, mem_value, mem_gate, gate_pre, forget_bias, forget_shift):
    row_count = mem_query.shape[0]
    head_count = forget_bias.shape[0]
    block_count = row_count // BLK
    sequence_total = row_count * lax.axis_size("sp")

    def blocks(array):
        return (
            array.astype(jnp.float32)
            .reshape(block_count, BLK, head_count, HD)
            .transpose(0, 2, 1, 3)
        )

    def gate_blocks(array):
        return array.reshape(block_count, BLK, head_count).transpose(0, 2, 1)

    log_in = gate_pre[:, 0, :] - 0.5 * math.log(sequence_total)
    log_forget = jax.nn.log_sigmoid(gate_pre[:, 1, :] + forget_bias) + forget_shift
    query_blocks = blocks(mem_query)
    key_blocks = blocks(mem_key) * HD ** (-0.5)
    value_blocks = blocks(mem_value)
    in_blocks = gate_blocks(log_in)
    forget_blocks = gate_blocks(log_forget)
    initial = (
        jnp.zeros((head_count, HD, HD), jnp.float32),
        jnp.zeros((head_count, HD), jnp.float32),
        jnp.full((head_count,), MASKED, jnp.float32),
    )

    def summarize(carried, block_data):
        key_block, value_block, in_block, forget_block = block_data
        return (
            advance(carried, key_block, value_block, in_block, jnp.cumsum(forget_block, axis=-1)),
            None,
        )

    summary, _ = lax.scan(summarize, initial, (key_blocks, value_blocks, in_blocks, forget_blocks))
    passed = jnp.sum(log_forget, axis=0)
    identity = (jnp.zeros((head_count,), jnp.float32), initial[0], initial[1], initial[2])
    incoming = entering((passed, summary[0], summary[1], summary[2]), "sp", join_states, identity)
    _, recall = lax.scan(
        block_step,
        (incoming[1], incoming[2], incoming[3]),
        (query_blocks, key_blocks, value_blocks, in_blocks, forget_blocks),
    )
    recall = recall.transpose(0, 2, 1, 3).reshape(row_count, head_count * HD)
    return (recall * jax.nn.sigmoid(mem_gate.astype(jnp.float32))).astype(jnp.bfloat16)


def shards(
    tokens,
    norm_gain,
    w_query,
    w_key,
    w_value,
    w_mem_query,
    w_mem_key,
    w_mem_value,
    w_mem_gate,
    w_gates,
    sinks,
    forget_bias,
    forget_shift,
    w_out,
):
    normed = normalize(tokens, norm_gain)
    token_rows = lax.all_gather(normed, "tp", axis=0, tiled=True)
    row_count = token_rows.shape[0]
    head_count = forget_bias.shape[0]
    gate_columns = lax.dynamic_slice_in_dim(
        w_gates, lax.axis_index("tp") * head_count, head_count, 2
    ).reshape(w_gates.shape[0], 2 * head_count)
    gate_pre = jnp.dot(token_rows, gate_columns, preferred_element_type=jnp.float32).reshape(
        row_count, 2, head_count
    )
    segments = (
        lax.all_gather(w_query, "sp", axis=0, tiled=True),
        lax.all_gather(w_key, "sp", axis=0, tiled=True),
        lax.all_gather(w_value, "sp", axis=0, tiled=True),
        lax.all_gather(w_mem_query, "sp", axis=0, tiled=True),
        lax.all_gather(w_mem_key, "sp", axis=0, tiled=True),
        lax.all_gather(w_mem_value, "sp", axis=0, tiled=True),
        lax.all_gather(w_mem_gate, "sp", axis=0, tiled=True),
    )
    columns = token_rows
    projected_sums = tuple(
        (jnp.dot(columns, segment, preferred_element_type=jnp.float32) for segment in segments)
    )
    projected = [partial_sum.astype(jnp.bfloat16) for partial_sum in projected_sums]
    attn_out, log_total = attend(projected[0], projected[1], projected[2], sinks)
    mem_parts = projected[3:]
    mem_out = memory(
        mem_parts[0], mem_parts[1], mem_parts[2], mem_parts[3], gate_pre, forget_bias, forget_shift
    )
    head_attn, head_mem = (
        lax.all_gather(attn_out, "tp", axis=1, tiled=True),
        lax.all_gather(mem_out, "tp", axis=1, tiled=True),
    )
    joined = jnp.concatenate([head_attn, head_mem], axis=1)
    columns = joined
    mixed = jnp.dot(
        columns, lax.all_gather(w_out, "sp", axis=0, tiled=True), preferred_element_type=jnp.float32
    )
    return (mixed.astype(jnp.bfloat16), log_total)


def solution(mesh):
    placed = (
        P(("sp", "tp"), None),
        P(),
        P("sp", "tp"),
        P("sp", "tp"),
        P("sp", "tp"),
        P("sp", "tp"),
        P("sp", "tp"),
        P("sp", "tp"),
        P("sp", "tp"),
        P(),
        P("tp"),
        P("tp"),
        P("sp", "tp"),
        P("sp", "tp"),
    )
    return jax.shard_map(
        shards,
        mesh=mesh,
        in_specs=placed,
        out_specs=(P("sp", "tp"), P("sp", "tp")),
        check_vma=False,
    )
```

profile of v0, /device:TPU:0, one launch (start us, length us, event | category | flops | bytes accessed | tf_op | source)
XLA Modules:
  0.0 535.0 jit_solution(10117530372503453236)
XLA Ops:
  9.4 2.3 fusion.51
  16.7 36.5 %all-gather.20.cloned.1.call-done = bf16[4096,128]{1,0:T(8,128)(2,1)} async-done(((bf16[512,128]{1,0:T(8,128)(2,1)}), bf16[4096,128]{1,0:T(8,128)(2,1)}) %all-gather.20.cloned.1.call-update) | async-done | bytes 1048592 | tf_op jit(solution)/shard_map/all_gather | solution.py:225
  53.2 29.4 %all-gather.16.cloned.1.call-done = bf16[384,4096]{1,0:T(8,128)(2,1)} async-done(((bf16[96,4096]{1,0:T(8,128)(2,1)}), bf16[384,4096]{1,0:T(8,128)(2,1)}) %all-gather.16.cloned.1.call-update) | async-done | bytes 3145744 | tf_op jit(solution)/shard_map/all_gather | solution.py:214
  82.5 3.3 convolution_convert_fusion.5
  87.1 3.4 collective-permute-start.1
  90.5 34.5 %all-gather.18.cloned.1.call-done = bf16[4096,128]{1,0:T(8,128)(2,1)} async-done(((bf16[512,128]{1,0:T(8,128)(2,1)}), bf16[4096,128]{1,0:T(8,128)(2,1)}) %all-gather.18.cloned.1.call-update) | async-done | bytes 1048592 | tf_op jit(solution)/shard_map/all_gather | solution.py:226
  125.0 2.2 convolution_convert_fusion.6
  127.2 1.7 reshape.294
  130.3 1.7 copy.59
  132.0 3.1 collective-permute-start
  135.1 1.7 copy.55
  138.3 1.7 reshape.293
  139.9 1.7 copy.58
  143.1 1.7 reshape.291
  144.7 1.7 copy.54
  146.4 52.4 %all-gather.22.cloned.1.call-done = bf16[4096,512]{1,0:T(8,128)(2,1)} async-done(((bf16[512,512]{1,0:T(8,128)(2,1)}), bf16[4096,512]{1,0:T(8,128)(2,1)}) %all-gather.22.cloned.1.call-update) | async-done | bytes 4194320 | tf_op jit(solution)/shard_map/all_gather | solution.py:224
  198.8 4.7 convolution_convert_fusion
  203.6 2.6 reshape.295
  206.2 2.0 fusion.44
  216.8 1.8 fusion.41
  219.2 29.3 %all-gather.26.cloned.1.call-done = bf16[4096,256]{1,0:T(8,128)(2,1)} async-done(((bf16[512,256]{1,0:T(8,128)(2,1)}), bf16[4096,256]{1,0:T(8,128)(2,1)}) %all-gather.26.cloned.1.call-update) | async-done | bytes 2097168 | tf_op jit(solution)/shard_map/all_gather | solution.py:229
  248.5 3.3 fusion.68
  251.9 1.9 copy.64
  253.8 1.9 reshape.263
  255.7 1.9 copy.66
  257.6 40.6 %all-gather.28.cloned.1.call-done = bf16[4096,256]{1,0:T(8,128)(2,1)} async-done(((bf16[512,256]{1,0:T(8,128)(2,1)}), bf16[4096,256]{1,0:T(8,128)(2,1)}) %all-gather.28.cloned.1.call-update) | async-done | bytes 2097168 | tf_op jit(solution)/shard_map/all_gather | solution.py:228
  298.2 3.3 fusion.67
  301.5 1.9 copy.65
  303.4 1.9 mul.176
  305.4 1.8 copy.67
  307.2 2.0 fusion.94
  309.2 22.4 %while.49 = (s32[]{:T(128)}, f32[4,64,64]{2,1,0:T(8,128)S(1)}, f32[4,64]{1,0:T(4,128)}, f32[4]{0:T(128)}, f32[3,4,128]{2,1,0:T(4,128)}, /*index=5*/f32[3,4,128]{...) while((s32[]{:T(128)}, f32[4,64,64]{2,1,0:T(8,128)S(1)}, ...), condition=%wide.region_7.8_spmd.clone, body=%wide.region_4.7_spmd.clone.sunk | while | flops 25709840 | bytes 552793 | solution.py:184
  333.8 19.3 %all-reduce.2 = (bf16[32]{0:T(256)(128)(2,1)S(1)}, bf16[32]{0:T(256)(128)(2,1)S(1)}) all-reduce(bf16[32]{0:T(256)(128)(2,1)} %copy-done.17, bf16[32]{0:T(256)(128)(2,1)} %copy-done.18), channel_id=2, replica_groups=mesh['sp'=8,'tp'=4] {'sp'}, use_global_device_ids=true, to_apply=%add | all-reduce | flops 64 | bytes 256
  353.9 34.9 %all-gather.2 = bf16[32,64,64]{2,1,0:T(8,128)(2,1)} all-gather(bf16[4,64,64]{2,1,0:T(8,128)(2,1)S(1)} %convert_element_type.114), channel_id=4, replica_groups=mesh['sp'=8,'tp'=4] {'sp'}, dimensions={0}, use_global_device_ids=true | all-gather | bytes 294912 | tf_op jit(solution)/shard_map/all_gather | solution.py:24
  389.4 17.3 %all-gather.4 = bf16[8,4,64]{2,1,0:T(4,128)(2,1)} all-gather(bf16[1,4,64]{2,1,0:T(4,128)(2,1)S(1)} %convert_bitcast_fusion), channel_id=5, replica_groups=mesh['sp'=8,'tp'=4] {'sp'}, dimensions={0}, use_global_device_ids=true | all-gather | bytes 4608 | tf_op jit(solution)/shard_map/all_gather | solution.py:24
  406.8 3.4 fusion.65
  410.3 1.9 copy.68
  412.2 1.9 reshape.264
  414.2 30.8 %while.48 = (s32[]{:T(128)}, f32[4,64,64]{2,1,0:T(8,128)S(1)}, f32[4,64]{1,0:T(4,128)S(1)}, f32[4]{0:T(128)S(1)}, f32[3,4,128,64]{2,3,1,0:T(8,128)}, /*index=5*/...) while((s32[]{:T(128)}, f32[4,64,64]{2,1,0:T(8,128)S(1)}, ...), condition=%wide.region_15.16_spmd, body=%wide.region_10.15_spmd.sunk | while | flops 152689152 | bytes 2546069 | solution.py:188
  419.9 1.9 fusion.163
  430.1 2.0 fusion.163
  440.4 1.9 fusion.163
  444.9 2.2 copy.95
  447.1 2.4 reshape.296
  449.5 2.6 fusion.64
  452.2 8.8 %all_gather.71 = bf16[384,1024]{1,0:T(8,128)(2,1)S(1)} all-gather(bf16[384,256]{1,0:T(8,128)(2,1)S(1)} %fusion.64), channel_id=1, replica_groups=mesh['sp'=8,'tp'=4] {'tp'}, dimensions={1}, use_global_device_ids=true | all-gather | bytes 983040 | tf_op jit(solution)/shard_map/all_gather | solution.py:244
  462.0 59.4 %all-gather.34.cloned.1.call-done = bf16[3072,1024]{1,0:T(8,128)(2,1)} async-done(((bf16[384,1024]{1,0:T(8,128)(2,1)}), bf16[3072,1024]{1,0:T(8,128)(2,1)}) %all-gather.34.cloned.1.call-update) | async-done | bytes 6291472 | tf_op jit(solution)/shard_map/all_gather | solution.py:249
  521.4 6.8 %fusion.53 = bf16[384,1024]{1,0:T(8,128)(2,1)} fusion(bf16[3072,1024]{1,0:T(8,128)(2,1)} %all-gather.34.cloned.1.call-done, bf16[384,1024]{0,1:T(8,128)(2,1)S(1)} %copy.74, bf16[384,2048]{0,1:T(8,128)(2,1)} %all-gather.24.cloned.1.call-done), kind=kOutput, calls=%fused_computation.92 | convolution fusion | flops 2421030912 | bytes 9437184 | tf_op jit(solution)/shard_map/dot_general | solution.py:248
  (182 shorter events, 73.0 us)
Async XLA Ops:
  7.2 204.8 %copy-start = (bf16[4096,2,16]{0,2,1:T(8,128)(2,1)S(1)}, bf16[4096,2,16]{0,2,1:T(8,128)(2,1)}, u32[]{:S(2)}) copy-start(bf16[4096,2,16]{0,2,1:T(8,128)(2,1)} %param.29) | copy-start | bytes 786436
  7.2 8.5 %copy-start.15 = (f32[8]{0:T(128)S(1)}, f32[8]{0:T(128)}, u32[]{:S(2)}) copy-start(f32[8]{0:T(128)} %param.30) | copy-start | bytes 100
  7.2 46.0 %all-gather.20.cloned.1.call-start = ((), (), s32[]{:S(2)}) async-start(), calls=%async_computation.2 | async-start | bytes 1179648 | tf_op jit(solution)/shard_map/all_gather | solution.py:225
  7.9 74.6 %all-gather.16.cloned.1.call-start = ((), (), s32[]{:S(2)}) async-start(), calls=%async_computation | async-start | bytes 3932160 | tf_op jit(solution)/shard_map/all_gather | solution.py:214
  11.7 113.3 %all-gather.18.cloned.1.call-start = ((), (), s32[]{:S(2)}) async-start(), calls=%async_computation.1 | async-start | bytes 1179648 | tf_op jit(solution)/shard_map/all_gather | solution.py:226
  12.4 186.4 %all-gather.22.cloned.1.call-start = ((), (), s32[]{:S(2)}) async-start(), calls=%async_computation.3 | async-start | bytes 4718592 | tf_op jit(solution)/shard_map/all_gather | solution.py:224
  13.0 235.5 %all-gather.26.cloned.1.call-start = ((), (), s32[]{:S(2)}) async-start(), calls=%async_computation.5 | async-start | bytes 2359296 | tf_op jit(solution)/shard_map/all_gather | solution.py:229
  13.6 284.6 %all-gather.28.cloned.1.call-start = ((), (), s32[]{:S(2)}) async-start(), calls=%async_computation.6 | async-start | bytes 2359296 | tf_op jit(solution)/shard_map/all_gather | solution.py:228
  14.2 392.7 %all-gather.30.cloned.1.call-start = ((), (), s32[]{:S(2)}) async-start(), calls=%async_computation.7 | async-start | bytes 2359296 | tf_op jit(solution)/shard_map/all_gather | solution.py:227
  14.9 434.6 %all-gather.32.cloned.1.call-start = ((), (), s32[]{:S(2)}) async-start(), calls=%async_computation.8 | async-start | bytes 2359296 | tf_op jit(solution)/shard_map/all_gather | solution.py:230
  15.7 446.4 %all-gather.24.cloned.1.call-start = ((), (), s32[]{:S(2)}) async-start(), calls=%async_computation.4 | async-start | bytes 1966080 | tf_op jit(solution)/shard_map/all_gather | solution.py:243
  15.8 193.2 %copy-start.12 = (f32[2,4]{1,0:T(2,128)}, f32[2,4]{1,0:T(2,128)S(1)}, u32[]{:S(2)}) copy-start(f32[2,4]{1,0:T(2,128)S(1)} %max.59) | copy-start | bytes 100
  82.5 42.4 %copy-start.1 = (bf16[384,4096]{1,0:T(8,128)(2,1)S(1)}, bf16[384,4096]{1,0:T(8,128)(2,1)}, u32[]{:S(2)}) copy-start(bf16[384,4096]{1,0:T(8,128)(2,1)} %all-gather.16.cloned.1.call-done) | copy-start | bytes 9437188
  85.8 0.6 copy-start.2
  87.1 49.7 %collective-permute-start.1 = (bf16[128,128]{1,0:T(8,128)(2,1)}, bf16[128,128]{1,0:T(8,128)(2,1)S(1)}, u32[]{:S(2)}, u32[]{:S(2)}) collective-permute-start(bf16[128,128]{1,0:T(8,128)(2,1)} %slice.50), channel_id=1, source_target_pairs={{0,4},{4,8},{8,12},{12,16},{16,20},{20,24},{24,28},{1,5},{5,9},{9,... | collective-permute-start | bytes 98312 | tf_op jit(solution)/shard_map/ppermute | solution.py:18
  132.0 9.6 %collective-permute-start = (bf16[128,128]{1,0:T(8,128)(2,1)}, bf16[128,128]{1,0:T(8,128)(2,1)}, u32[]{:S(2)}, u32[]{:S(2)}) collective-permute-start(bf16[128,128]{1,0:T(8,128)(2,1)} %slice.49), channel_id=1, source_target_pairs={{0,4},{4,8},{8,12},{12,16},{16,20},{20,24},{24,28},{1,5},{5,9},{9,... | collective-permute-start | bytes 98312 | tf_op jit(solution)/shard_map/ppermute | solution.py:18
  146.4 59.8 %copy-start.3 = (pred[3,128,256]{1,2,0:T(8,128)(4,1)S(1)}, pred[3,128,256]{1,2,0:T(8,128)(4,1)}, u32[]{:S(2)}) copy-start(pred[3,128,256]{1,2,0:T(8,128)(4,1)} %fusion.71) | copy-start | bytes 294916
  206.2 2.9 copy-start.9
  206.2 2.9 copy-start.10
  208.3 1.8 copy-start.7
  209.0 1.1 copy-start.5
  210.1 5.5 %copy-start.16 = (u32[32]{0:T(128)S(1)}, u32[32]{0:T(128)}, u32[]{:S(2)}) copy-start(u32[32]{0:T(128)} %constant.110) | copy-start | bytes 388
  211.3 310.1 %all-gather.34.cloned.1.call-start = ((), (), s32[]{:S(2)}) async-start(), calls=%async_computation.9 | async-start | bytes 7077888 | tf_op jit(solution)/shard_map/all_gather | solution.py:249
  218.6 0.6 copy-start.11
  257.6 49.6 %copy-start.14 = (f32[4]{0:T(128)S(1)}, f32[4]{0:T(128)}, u32[]{:S(2)}) copy-start(f32[4]{0:T(128)} %param.31) | copy-start | bytes 52
  331.6 75.2 %copy-start.4 = (f32[3,4,128]{2,1,0:T(4,128)}, f32[3,4,128]{2,1,0:T(4,128)S(1)}, u32[]{:S(2)}) copy-start(f32[3,4,128]{2,1,0:T(4,128)S(1)} %get-tuple-element.643) | copy-start | bytes 18436
  332.4 0.9 copy-start.18
  333.3 0.5 copy-start.17
  449.5 11.8 %copy-start.6 = (f32[3,2,4,128]{3,2,1,0:T(4,128)S(1)}, f32[3,2,4,128]{3,2,1,0:T(4,128)}, u32[]{:S(2)}) copy-start(f32[3,2,4,128]{3,2,1,0:T(4,128)} %copy-done.5) | copy-start | bytes 36868
  449.5 11.8 %copy-start.8 = (f32[3,2,4,128]{3,2,1,0:T(4,128)S(1)}, f32[3,2,4,128]{3,2,1,0:T(4,128)}, u32[]{:S(2)}) copy-start(f32[3,2,4,128]{3,2,1,0:T(4,128)} %copy-done.7) | copy-start | bytes 36868
  449.5 11.8 %copy-start.13 = (f32[2,4]{1,0:T(2,128)S(1)}, f32[2,4]{1,0:T(2,128)}, u32[]{:S(2)}) copy-start(f32[2,4]{1,0:T(2,128)} %copy-done.12) | copy-start | bytes 100
Sparse Core Ops, SparseCore 0:
  10.1 42.9 all-gather.19
  55.3 27.2 all-gather.15
  84.7 40.2 all-gather.17
  127.0 71.8 all-gather.21
  200.8 47.6 all-gather.25
  250.5 47.6 all-gather.27
  300.3 47.9 all-gather.29
  350.4 49.6 all-gather.31
  401.6 18.9 all-gather.23
  422.6 98.7 all-gather.33
where the time goes:
time: 538 us; the launch traced here: 535 us
  waiting for transfers between devices  287 us (53%)
  blocking collectives  80.3 us (15%)
  matrix products  61.6 us (11%)
  local copies, waits for them, and re-layouts  54.6 us (10%)
  other arithmetic  29.4 us (5%)
  between operations  15.1 us (3%)
  starting transfers between devices  7 us (1%)
    all_gather x1, waiting for transfers between devices, shards(): lax.all_gather(w_out, 'sp', axis=0, tiled=True)  59.4 us
    all_gather x1, waiting for transfers between devices, shards(): lax.all_gather(w_query, 'sp', axis=0, tiled=True)  52.4 us
    all_gather x2, blocking collectives, entering(): lax.all_gather(a.astype(kind), axis)  52.2 us
    all_gather x1, waiting for transfers between devices, shards(): lax.all_gather(w_mem_key, 'sp', axis=0, tiled=True)  40.6 us
    all_gather x1, waiting for transfers between devices, shards(): lax.all_gather(w_key, 'sp', axis=0, tiled=True)  36.5 us
    all_gather x1, waiting for transfers between devices, shards(): lax.all_gather(w_value, 'sp', axis=0, tiled=True)  34.5 us
    all_gather x1, waiting for transfers between devices, shards(): token_rows = lax.all_gather(normed, 'tp', axis=0, tiled=True)  29.4 us
    all_gather x1, waiting for transfers between devices, shards(): lax.all_gather(w_mem_value, 'sp', axis=0, tiled=True)  29.3 us
  transfers between devices with their start and end apart: 12, of which 7 were waited for; matrix products, arithmetic and copies ran while one was open for 26% of the time, Pallas kernels for 0%

commit v1 on v0

--- a/solution.py
+++ b/solution.py
@@ -211,7 +211,12 @@
     w_out,
 ):
     normed = normalize(tokens, norm_gain)
-    token_rows = lax.all_gather(normed, "tp", axis=0, tiled=True)
+    ring = [normed]
+    for hop in range(3):
+        ring.append(lax.ppermute(ring[-1], "tp", [(dev, (dev + 1) % 4) for dev in range(4)]))
+    token_rows = jnp.roll(
+        jnp.concatenate(ring[::-1], axis=0), (lax.axis_index("tp") + 1) * ring[0].shape[0], axis=0
+    )
     row_count = token_rows.shape[0]
     head_count = forget_bias.shape[0]
     gate_columns = lax.dynamic_slice_in_dim(

time: 538 us -> 505 us (0.939)
  waiting for transfers between devices: 287 us -> 331 us
  local copies, waits for them, and re-layouts: 54.6 us -> 13.6 us
  other arithmetic: 29.4 us -> 12.2 us
  matrix products: 61.6 us -> 45.3 us
    all_gather x1, waiting for transfers between devices: 59.4 us -> 99.8 us  [shards(): lax.all_gather(w_out, 'sp', axis=0, tiled=True)]
    all_gather x1, waiting for transfers between devices: 36.5 us -> 0.01 us  [shards(): lax.all_gather(w_key, 'sp', axis=0, tiled=True)]
    ppermute x0 -> x3, waiting for transfers between devices: none -> 34 us  [shards(): lax.ppermute(ring[-1], 'tp', [(dev, (dev + 1) % 4) for dev in range(4)])]
    all_gather x1 -> x0, waiting for transfers between devices: 29.4 us -> none  [shards(): token_rows = lax.all_gather(normed, 'tp', axis=0, tiled=True)]
    all_gather x1, waiting for transfers between devices: 52.4 us -> 65.7 us  [shards(): lax.all_gather(w_query, 'sp', axis=0, tiled=True)]
    all_gather x1, waiting for transfers between devices: 0.01 us -> 9.8 us  [shards(): lax.all_gather(w_mem_gate, 'sp', axis=0, tiled=True)]
    transpose x4, local copies, waits for them, and re-layouts: 7.74 us -> 0.64 us  [blocks(): return array.astype(jnp.float32).reshape(block_count, BLK, head_count, HD...]
    slice x4, local copies, waits for them, and re-layouts: 6.76 us -> 0.52 us  [attend(): key_window = jnp.concatenate([padded_keys[:-1], padded_keys[1:]], axis=1)]
  transfers between devices with their start and end apart: 12 -> 14, of which waited for: 7 -> 11; matrix products, arithmetic and copies ran while one was open for 26% -> 13% of each run, Pallas kernels for 0% -> 0%
where the time goes in v1:
time: 505 us
  waiting for transfers between devices  331 us (66%)
  blocking collectives  79.3 us (16%)
  matrix products  45.3 us (9%)
  between operations  15 us (3%)
  local copies, waits for them, and re-layouts  13.6 us (3%)
  other arithmetic  12.2 us (2%)
  starting transfers between devices  7.8 us (2%)
    all_gather x1, waiting for transfers between devices, shards(): lax.all_gather(w_out, 'sp', axis=0, tiled=True)  99.8 us
    all_gather x1, waiting for transfers between devices, shards(): lax.all_gather(w_query, 'sp', axis=0, tiled=True)  65.7 us
    all_gather x2, blocking collectives, entering(): lax.all_gather(a.astype(kind), axis)  51.2 us
    all_gather x1, waiting for transfers between devices, shards(): lax.all_gather(w_mem_key, 'sp', axis=0, tiled=True)  45.7 us
    all_gather x1, waiting for transfers between devices, shards(): lax.all_gather(w_mem_value, 'sp', axis=0, tiled=True)  35.1 us
    ppermute x3, waiting for transfers between devices, shards(): lax.ppermute(ring[-1], 'tp', [(dev, (dev + 1) % 4) for dev in range(4)])  34 us
    all_gather x1, waiting for transfers between devices, shards(): lax.all_gather(w_value, 'sp', axis=0, tiled=True)  29.7 us
    dot_general x7, matrix products, shards(): jnp.dot(columns, segment, preferred_element_type=jnp.float32)  25.5 us
  transfers between devices with their start and end apart: 14, of which 11 were waited for; matrix products, arithmetic and copies ran while one was open for 13% of the time, Pallas kernels for 0%

profile of v1, /device:TPU:0, one launch (start us, length us, event | category | flops | bytes accessed | tf_op | source)
XLA Modules:
  0.0 505.0 jit_solution(6668782783983865761)
XLA Ops:
  7.2 0.7 all-gather.17.cloned.1.call-update
  8.0 0.7 all-gather.15.cloned.1.call-update
  8.7 0.7 all-gather.19.cloned.1.call-update
  11.2 1.4 fusion.49
  12.6 1.5 fusion.51
  14.6 11.6 %collective-permute-done = bf16[96,4096]{1,0:T(8,128)(2,1)S(1)} collective-permute-done((bf16[96,4096]{1,0:T(8,128)(2,1)S(1)}, bf16[96,4096]{1,0:T(8,128)(2,1)S(1)}, u32[]{:S(2)}, u32[]{:S(2)}) %collective-permute-start) | collective-permute-done | bytes 786464 | tf_op jit(solution)/shard_map/ppermute | solution.py:216
  26.2 11.4 %collective-permute-done.1 = bf16[96,4096]{1,0:T(8,128)(2,1)S(1)} collective-permute-done((bf16[96,4096]{1,0:T(8,128)(2,1)S(1)}, bf16[96,4096]{1,0:T(8,128)(2,1)S(1)}, u32[]{:S(2)}, u32[]{:S(2)}) %collective-permute-start.1) | collective-permute-done | bytes 786464 | tf_op jit(solution)/shard_map/ppermute | solution.py:216
  38.0 11.0 %collective-permute-done.2 = bf16[96,4096]{1,0:T(8,128)(2,1)S(1)} collective-permute-done((bf16[96,4096]{1,0:T(8,128)(2,1)S(1)}, bf16[96,4096]{1,0:T(8,128)(2,1)S(1)}, u32[]{:S(2)}, u32[]{:S(2)}) %collective-permute-start.2) | collective-permute-done | bytes 786464 | tf_op jit(solution)/shard_map/ppermute | solution.py:216
  49.1 1.0 constant_dynamic-update-slice_fusion.7
  50.0 0.9 constant_dynamic-update-slice_fusion.6
  51.0 1.0 constant_dynamic-update-slice_fusion.5
  52.0 1.2 constant_dynamic-update-slice_fusion.4
  53.2 0.9 constant_dynamic-update-slice_fusion.3
  54.2 1.0 constant_dynamic-update-slice_fusion.2
  55.1 0.9 constant_dynamic-update-slice_fusion.1
  56.1 1.2 constant_dynamic-update-slice_fusion
  57.2 3.2 convolution_convert_fusion.5
  60.4 4.2 collective-permute-start.4
  64.7 29.7 %all-gather.15.cloned.1.call-done = bf16[4096,128]{1,0:T(8,128)(2,1)} async-done(((bf16[512,128]{1,0:T(8,128)(2,1)}), bf16[4096,128]{1,0:T(8,128)(2,1)}) %all-gather.15.cloned.1.call-update) | async-done | bytes 1048592 | tf_op jit(solution)/shard_map/all_gather | solution.py:231
  94.4 3.2 convolution_convert_fusion.6
  98.0 2.5 collective-permute-start.3
  100.9 1.1 collective-permute-done.3
  102.3 65.7 %all-gather.19.cloned.1.call-done = bf16[4096,512]{1,0:T(8,128)(2,1)} async-done(((bf16[512,512]{1,0:T(8,128)(2,1)}), bf16[4096,512]{1,0:T(8,128)(2,1)}) %all-gather.19.cloned.1.call-update) | async-done | bytes 4194320 | tf_op jit(solution)/shard_map/all_gather | solution.py:229
  168.1 5.0 convolution_convert_fusion
  173.4 0.7 fusion.44
  174.2 0.7 fusion.43
  175.0 0.9 fusion.57
  176.3 0.8 copy.104
  179.3 2.8 fusion.41
  182.6 35.1 %all-gather.23.cloned.1.call-done = bf16[4096,256]{1,0:T(8,128)(2,1)} async-done(((bf16[512,256]{1,0:T(8,128)(2,1)}), bf16[4096,256]{1,0:T(8,128)(2,1)}) %all-gather.23.cloned.1.call-update) | async-done | bytes 2097168 | tf_op jit(solution)/shard_map/all_gather | solution.py:234
  217.8 3.5 fusion.68
  221.7 45.7 %all-gather.25.cloned.1.call-done = bf16[4096,256]{1,0:T(8,128)(2,1)} async-done(((bf16[512,256]{1,0:T(8,128)(2,1)}), bf16[4096,256]{1,0:T(8,128)(2,1)}) %all-gather.25.cloned.1.call-update) | async-done | bytes 2097168 | tf_op jit(solution)/shard_map/all_gather | solution.py:233
  267.4 3.5 fusion.67
  271.3 4.6 while.49
  276.0 32.9 %all-gather.2 = bf16[32,64,64]{2,1,0:T(8,128)(2,1)S(1)} all-gather(bf16[4,64,64]{2,1,0:T(8,128)(2,1)S(1)} %convert_element_type.114), channel_id=4, replica_groups=mesh['sp'=8,'tp'=4] {'sp'}, dimensions={0}, use_global_device_ids=true | all-gather | bytes 294912 | tf_op jit(solution)/shard_map/all_gather | solution.py:24
  309.1 18.3 %all-gather.4 = bf16[8,4,64]{2,1,0:T(4,128)(2,1)S(1)} all-gather(bf16[1,4,64]{2,1,0:T(4,128)(2,1)S(1)} %convert_bitcast_fusion), channel_id=5, replica_groups=mesh['sp'=8,'tp'=4] {'sp'}, dimensions={0}, use_global_device_ids=true | all-gather | bytes 4608 | tf_op jit(solution)/shard_map/all_gather | solution.py:24
  327.5 17.6 %all-reduce.2 = (bf16[32]{0:T(256)(128)(2,1)S(1)}, bf16[32]{0:T(256)(128)(2,1)S(1)}) all-reduce(bf16[32]{0:T(256)(128)(2,1)S(1)} %dynamic-update-slice, bf16[32]{0:T(256)(128)(2,1)S(1)} %dynamic-update-slice.1), channel_id=2, replica_groups=mesh['sp'=8,'tp'=4] {'sp'}, use_global_device_ids=true, to_apply=%add | all-reduce | flops 64 | bytes 256
  345.3 3.6 fusion.65
  349.2 10.6 %while.48 = (s32[]{:T(128)}, f32[4,64,64]{2,1,0:T(8,128)S(1)}, f32[4,64]{1,0:T(4,128)S(1)}, f32[4]{0:T(128)S(1)}, f32[3,4,128,64]{2,3,1,0:T(8,128)S(1)}, /*index...) while((s32[]{:T(128)}, f32[4,64,64]{2,1,0:T(8,128)S(1)}, ...), condition=%wide.region_15.16_spmd, body=%wide.region_10.15_spmd.sunk | while | flops 152689152 | bytes 2611085 | solution.py:188
  350.3 0.7 fusion.169
  353.9 0.7 fusion.169
  360.6 9.8 %all-gather.29.cloned.1.call-done = bf16[4096,256]{1,0:T(8,128)(2,1)} async-done(((bf16[512,256]{1,0:T(8,128)(2,1)}), bf16[4096,256]{1,0:T(8,128)(2,1)}) %all-gather.29.cloned.1.call-update) | async-done | bytes 2097168 | tf_op jit(solution)/shard_map/all_gather | solution.py:235
  370.4 3.6 fusion.64
  374.0 10.6 %all_gather.67 = bf16[384,1024]{1,0:T(8,128)(2,1)S(1)} all-gather(bf16[384,256]{1,0:T(8,128)(2,1)S(1)} %fusion.64), channel_id=1, replica_groups=mesh['sp'=8,'tp'=4] {'tp'}, dimensions={1}, use_global_device_ids=true | all-gather | bytes 983040 | tf_op jit(solution)/shard_map/all_gather | solution.py:249
  384.9 0.7 fusion.88
  385.6 6.2 %all-gather.21.cloned.1.call-done = bf16[384,2048]{0,1:T(8,128)(2,1)} async-done(((bf16[384,512]{0,1:T(8,128)(2,1)}), bf16[384,2048]{0,1:T(8,128)(2,1)}) %all-gather.21.cloned.1.call-update) | async-done | bytes 1572880 | tf_op jit(solution)/shard_map/all_gather | solution.py:248
  391.8 99.8 %all-gather.31.cloned.1.call-done = bf16[3072,1024]{1,0:T(8,128)(2,1)} async-done(((bf16[384,1024]{1,0:T(8,128)(2,1)}), bf16[3072,1024]{1,0:T(8,128)(2,1)}) %all-gather.31.cloned.1.call-update) | async-done | bytes 6291472 | tf_op jit(solution)/shard_map/all_gather | solution.py:254
  491.6 6.8 %fusion.53 = bf16[384,1024]{1,0:T(8,128)(2,1)} fusion(bf16[3072,1024]{1,0:T(8,128)(2,1)} %all-gather.31.cloned.1.call-done, bf16[384,1024]{0,1:T(8,128)(2,1)S(1)} %copy.74, bf16[384,2048]{0,1:T(8,128)(2,1)} %all-gather.21.cloned.1.call-done), kind=kOutput, calls=%fused_computation.92 | convolution fusion | flops 2421030912 | bytes 9437184 | tf_op jit(solution)/shard_map/dot_general | solution.py:253
  (169 shorter events, 23.0 us)
Async XLA Ops:
  7.2 170.8 %copy-start = (bf16[4096,2,16]{0,2,1:T(8,128)(2,1)S(1)}, bf16[4096,2,16]{0,2,1:T(8,128)(2,1)}, u32[]{:S(2)}) copy-start(bf16[4096,2,16]{0,2,1:T(8,128)(2,1)} %param.29) | copy-start | bytes 786436
  7.2 30.6 %copy-start.5 = (f32[8]{0:T(128)S(1)}, f32[8]{0:T(128)}, u32[]{:S(2)}) copy-start(f32[8]{0:T(128)} %param.30) | copy-start | bytes 100
  7.2 50.0 %all-gather.17.cloned.1.call-start = ((), (), s32[]{:S(2)}) async-start(), calls=%async_computation.1 | async-start | bytes 1179648 | tf_op jit(solution)/shard_map/all_gather | solution.py:230
  7.9 86.5 %all-gather.15.cloned.1.call-start = ((), (), s32[]{:S(2)}) async-start(), calls=%async_computation | async-start | bytes 1179648 | tf_op jit(solution)/shard_map/all_gather | solution.py:231
  8.7 159.4 %all-gather.19.cloned.1.call-start = ((), (), s32[]{:S(2)}) async-start(), calls=%async_computation.2 | async-start | bytes 4718592 | tf_op jit(solution)/shard_map/all_gather | solution.py:229
  9.4 208.4 %all-gather.23.cloned.1.call-start = ((), (), s32[]{:S(2)}) async-start(), calls=%async_computation.4 | async-start | bytes 2359296 | tf_op jit(solution)/shard_map/all_gather | solution.py:234
  10.0 257.4 %all-gather.25.cloned.1.call-start = ((), (), s32[]{:S(2)}) async-start(), calls=%async_computation.5 | async-start | bytes 2359296 | tf_op jit(solution)/shard_map/all_gather | solution.py:233
  10.6 334.7 %all-gather.27.cloned.1.call-start = ((), (), s32[]{:S(2)}) async-start(), calls=%async_computation.6 | async-start | bytes 2359296 | tf_op jit(solution)/shard_map/all_gather | solution.py:232
  11.1 359.3 %all-gather.29.cloned.1.call-start = ((), (), s32[]{:S(2)}) async-start(), calls=%async_computation.7 | async-start | bytes 2359296 | tf_op jit(solution)/shard_map/all_gather | solution.py:235
  12.6 39.4 %copy-start.1 = (bf16[96,4096]{1,0:T(8,128)(2,1)S(1)}, bf16[96,4096]{1,0:T(8,128)(2,1)}, u32[]{:S(2)}) copy-start(bf16[96,4096]{1,0:T(8,128)(2,1)} %param.20) | copy-start | bytes 2359300
  12.6 39.4 %copy-start.2 = (f32[4096]{0:T(1024)S(1)}, f32[4096]{0:T(1024)}, u32[]{:S(2)}) copy-start(f32[4096]{0:T(1024)} %param.21) | copy-start | bytes 49156
  14.1 12.1 %collective-permute-start = (bf16[96,4096]{1,0:T(8,128)(2,1)S(1)}, bf16[96,4096]{1,0:T(8,128)(2,1)S(1)}, u32[]{:S(2)}, u32[]{:S(2)}) collective-permute-start(bf16[96,4096]{1,0:T(8,128)(2,1)S(1)} %fusion.51), channel_id=1, source_target_pairs={{0,1},{1,2},{2,3},{3,0},{4,5},{5,6},{6,7},{7,4},{8,9},{9,10},{10,1... | collective-permute-start | bytes 2359304 | tf_op jit(solution)/shard_map/ppermute | solution.py:216
  26.2 11.4 %collective-permute-start.1 = (bf16[96,4096]{1,0:T(8,128)(2,1)S(1)}, bf16[96,4096]{1,0:T(8,128)(2,1)S(1)}, u32[]{:S(2)}, u32[]{:S(2)}) collective-permute-start(bf16[96,4096]{1,0:T(8,128)(2,1)S(1)} %collective-permute-done), channel_id=1, source_target_pairs={{0,1},{1,2},{2,3},{3,0},{4,5},{5,6},{6,7},{7,4},{8,9},{9,10},{10,1... | collective-permute-start | bytes 2359304 | tf_op jit(solution)/shard_map/ppermute | solution.py:216
  37.6 11.4 %collective-permute-start.2 = (bf16[96,4096]{1,0:T(8,128)(2,1)S(1)}, bf16[96,4096]{1,0:T(8,128)(2,1)S(1)}, u32[]{:S(2)}, u32[]{:S(2)}) collective-permute-start(bf16[96,4096]{1,0:T(8,128)(2,1)S(1)} %collective-permute-done.1), channel_id=1, source_target_pairs={{0,1},{1,2},{2,3},{3,0},{4,5},{5,6},{6,7},{7,4},{8,9},{9,10},{10,1... | collective-permute-start | bytes 2359304 | tf_op jit(solution)/shard_map/ppermute | solution.py:216
  37.7 354.1 %all-gather.21.cloned.1.call-start = ((), (), s32[]{:S(2)}) async-start(), calls=%async_computation.3 | async-start | bytes 1966080 | tf_op jit(solution)/shard_map/all_gather | solution.py:248
  60.4 40.2 %collective-permute-start.4 = (bf16[128,128]{1,0:T(8,128)(2,1)S(1)}, bf16[128,128]{1,0:T(8,128)(2,1)S(1)}, u32[]{:S(2)}, u32[]{:S(2)}) collective-permute-start(bf16[128,128]{1,0:T(8,128)(2,1)S(1)} %slice.50), channel_id=1, source_target_pairs={{0,4},{4,8},{8,12},{12,16},{16,20},{20,24},{24,28},{1,5},{5,9},{9,... | collective-permute-start | bytes 98312 | tf_op jit(solution)/shard_map/ppermute | solution.py:18
  98.0 4.1 collective-permute-start.3
  175.9 2.1 copy-start.6
  175.9 6.2 %copy-start.3 = (f32[384,4]{0,1:T(4,128)S(1)}, f32[384,4]{0,1:T(4,128)}, u32[]{:S(2)}) copy-start(f32[384,4]{0,1:T(4,128)} %param.32) | copy-start | bytes 18436
  176.0 6.2 %copy-start.4 = (f32[4]{0:T(128)S(1)}, f32[4]{0:T(128)}, u32[]{:S(2)}) copy-start(f32[4]{0:T(128)} %param.31) | copy-start | bytes 52
  177.1 314.5 %all-gather.31.cloned.1.call-start = ((), (), s32[]{:S(2)}) async-start(), calls=%async_computation.8 | async-start | bytes 7077888 | tf_op jit(solution)/shard_map/all_gather | solution.py:254
Sparse Core Ops, SparseCore 0:
  10.1 42.9 all-gather.16
  55.3 39.0 all-gather.14
  96.5 71.4 all-gather.18
  170.0 47.6 all-gather.22
  219.7 47.6 all-gather.24
  269.4 49.8 all-gather.26
  321.4 48.9 all-gather.28
  372.5 19.2 all-gather.20
  394.0 97.6 all-gather.30
